TPU v7x, 512 devices: a whole 4x4x16 slice. The times are simulated.
512 devices in a mesh: ep: 32 (over z, core), tp: 16 (over y, x).
Axes of the slice: x: 4, y: 4, z: 16, core: 2. Of those that a mesh axis runs over, the one named last changes fastest.
Arguments:
- mixer_rows: bfloat16 [16384, 2048], P('ep', 'tp'), may hold values from -6 to 6
- expert_rows: bfloat16 [16384, 2048], P('ep', 'tp'), may hold values from -6 to 6
- mixer_gain: float32 [2048], replicated, may hold values from 0.1 to 1.9
- pool_scale: float32 [2048], P('tp'), may hold values from 0.1 to 1.9
- w_in: bfloat16 [2048, 2048], P(None, 'tp'), may hold values from -0.125 to 0.125
- w_mix_out: bfloat16 [2048, 2048], P(None, 'tp'), may hold values from -0.125 to 0.125
- expert_gain: float32 [2048], replicated, may hold values from 0.1 to 1.9
- expert_gate: bfloat16 [32, 2048, 2048], P('ep', None, 'tp'), may hold values from -0.125 to 0.125
- expert_up: bfloat16 [32, 2048, 2048], P('ep', None, 'tp'), may hold values from -0.125 to 0.125
- expert_down: bfloat16 [32, 2048, 2048], P('ep', None, 'tp'), may hold values from -0.125 to 0.125
- routes: int32 [16384, 2], P('ep'), may hold values from 0 to 31, all different within a row; in each aligned block of 512 rows (0 to 511, 512 to 1023, ...) at most 48 rows name the same one
- route_weight: float32 [16384, 2], P('ep'), may hold values from 0.1 to 1
Outputs:
- mixer_output: bfloat16 [16384, 2048], P('ep', 'tp')
- expert_output: bfloat16 [16384, 2048], P('ep', 'tp')
Inputs may be any that keep to these rules, and one draw needn't show every extreme that they name: `routes`: each row names 2 different experts. Among the rows of one device (aligned blocks of 512 rows) no expert is named more than 48 times, a bound that some block reaches.
All inputs are finite; a program needn't handle non-finite values.
Results may differ from a plain program's by a relative error of at most 0.0071.
Values may be sent and summed in bfloat16 or wider, within the bound.
A program may use at most 64 MiB of HBM per device.

v0:
```python
import jax
import jax.numpy as jnp
from jax import lax
from jax.sharding import PartitionSpec as P

PW = 2048
TOP = 2


norm_eps = 1e-05
pool_windows = (2, 4, 8, 16)
rim_rows = 8


def extended_2(block, sides, width):
    for axis, dim in sides:
        count = lax.axis_size(axis)
        forward = [(i, i + 1) for i in range(count - 1)]
        backward = [(target, source) for source, target in forward]
        low = lax.ppermute(
            lax.slice_in_dim(block, block.shape[dim] - width, None, axis=dim), axis, forward
        )
        high = lax.ppermute(lax.slice_in_dim(block, 0, width, axis=dim), axis, backward)
        block = jnp.concatenate([low, block, high], axis=dim)
    return block


def laid_out(parts, dim):
    dims = list(parts.shape[1:])
    dims[dim] *= parts.shape[0]
    return jnp.moveaxis(parts, 0, dim).reshape(dims)


def sent_to_all(array, axis):
    length = lax.axis_size(axis)
    return lax.all_to_all(
        jnp.broadcast_to(array[None], (length, *array.shape)), axis, 0, 0, tiled=True
    )


def collect(array, axis, dim):
    return laid_out(sent_to_all(array, axis), dim)


def side_by_side(arrays, axis, dim, along):
    ends, at = ([], 0)
    for a in arrays[:-1]:
        at += a.shape[along]
        ends.append(at)
    both = jnp.concatenate(arrays, axis=along)
    return tuple(jnp.split(lax.all_gather(both, axis, axis=dim, tiled=True), ends, axis=along))


def layer_norm(row_block, gain_vec):
    values = row_block.astype(jnp.float32)
    center = values - jnp.mean(values, axis=-1, keepdims=True)
    spread = jnp.mean(center * center, axis=-1, keepdims=True)
    return (center * lax.rsqrt(spread + norm_eps) * gain_vec).astype(jnp.bfloat16)


def pooled_channels(inner_t, scale_local, ep_size, ep_index, tp_index):
    extended = extended_2(inner_t, (("ep", 1),), rim_rows).astype(jnp.float32)
    values = inner_t.astype(jnp.float32)
    channels = values.shape[0]
    row_count = values.shape[1]
    seq_len = row_count * ep_size
    position = ep_index * row_count + jnp.arange(row_count, dtype=jnp.int32)
    channel = tp_index * channels + jnp.arange(channels, dtype=jnp.int32)
    group = channel // (PW // 4)
    running = jnp.zeros((channels, row_count), jnp.float32)
    result = jnp.zeros((channels, row_count), jnp.float32)
    last_half = 0
    for group_id, window in enumerate(pool_windows):
        half_span = window // 2
        for offset in list(range(-half_span, -last_half)) + list(range(last_half, half_span)):
            running = running + extended[:, rim_rows + offset : rim_rows + offset + row_count]
        last_half = half_span
        lower_end = jnp.clip(position - half_span, 0, seq_len)
        upper_end = jnp.clip(position - half_span + window, 0, seq_len)
        counts = (upper_end - lower_end).astype(jnp.float32)
        member = (group == group_id)[:, None]
        result = jnp.where(member, running / counts[None, :], result)
    return ((result - values) * scale_local[:, None]).astype(jnp.bfloat16)


def on_device(
    mixer_rows,
    expert_rows,
    mixer_gain,
    pool_scale,
    w_in,
    w_mix_out,
    expert_gain,
    expert_gate,
    expert_up,
    expert_down,
    routes,
    route_weight,
):
    ep_size = lax.axis_size("ep")
    ep_index = lax.axis_index("ep")
    tp_index = lax.axis_index("tp")
    row_count = routes.shape[0]
    capacity = (3 * TOP * row_count + 2 * ep_size - 1) // (2 * ep_size)
    flat_route = routes.reshape(-1)
    onehot = (flat_route[:, None] == jnp.arange(ep_size, dtype=jnp.int32)[None, :]).astype(
        jnp.int32
    )
    ranking = jnp.sum(onehot * (jnp.cumsum(onehot, axis=0) - 1), axis=1)
    target = flat_route * capacity + ranking
    sender = (
        jnp.zeros((ep_size * capacity,), jnp.int32)
        .at[target]
        .set(jnp.arange(row_count * TOP, dtype=jnp.int32) // TOP + 1)
    )
    filled = (sender > 0)[:, None]
    source_row = jnp.maximum(sender - 1, 0)
    full_mix = collect(mixer_rows, "tp", 1)
    feature_count = expert_rows.shape[1]
    outgoing = jnp.where(filled, expert_rows[source_row], jnp.zeros((), jnp.bfloat16))
    arrived = lax.all_to_all(
        outgoing.reshape(ep_size, capacity, feature_count),
        "ep",
        split_axis=0,
        concat_axis=0,
        tiled=True,
    )
    slot_slices = arrived.reshape(ep_size * capacity, feature_count)
    slot_normed = layer_norm(lax.all_gather(slot_slices, "tp", axis=1, tiled=True), expert_gain)
    contract_first = (((0,), (1,)), ((), ()))
    normed_mix = layer_norm(full_mix, mixer_gain)
    inner_t = lax.dot_general(
        w_in, normed_mix, contract_first, preferred_element_type=jnp.float32
    ).astype(jnp.bfloat16)
    pooled_t = pooled_channels(inner_t, pool_scale, ep_size, ep_index, tp_index)
    gate_t = lax.dot_general(
        expert_gate[0], slot_normed, contract_first, preferred_element_type=jnp.float32
    )
    up_t = lax.dot_general(
        expert_up[0], slot_normed, contract_first, preferred_element_type=jnp.float32
    )
    hidden_t = (jax.nn.silu(gate_t) * up_t).astype(jnp.bfloat16)
    contract_lead = (((0,), (0,)), ((), ()))
    pieces = side_by_side((pooled_t, hidden_t), "tp", 0, 1)
    down_weight = expert_down[0]
    mixed_sum = lax.dot_general(
        pieces[0], w_mix_out, contract_lead, preferred_element_type=jnp.float32
    )
    expert_sum = lax.dot_general(
        pieces[1], down_weight, contract_lead, preferred_element_type=jnp.float32
    )
    mixer_output = mixed_sum.astype(jnp.bfloat16)
    back_rows = expert_sum.astype(jnp.bfloat16).reshape(ep_size, capacity, expert_sum.shape[1])
    returned = lax.all_to_all(back_rows, "ep", split_axis=0, concat_axis=0, tiled=True).reshape(
        ep_size * capacity, expert_sum.shape[1]
    )
    picked = returned[target].astype(jnp.float32).reshape(row_count, TOP, expert_sum.shape[1])
    expert_output = jnp.sum(picked * route_weight[:, :, None], axis=1).astype(jnp.bfloat16)
    return (mixer_output, expert_output)


def solution(mesh):
    return jax.shard_map(
        on_device,
        mesh=mesh,
        in_specs=(
            P("ep", "tp"),
            P("ep", "tp"),
            P(),
            P("tp"),
            P(None, "tp"),
            P(None, "tp"),
            P(),
            P("ep", None, "tp"),
            P("ep", None, "tp"),
            P("ep", None, "tp"),
            P("ep", None),
            P("ep", None),
        ),
        out_specs=(P("ep", "tp"), P("ep", "tp")),
        check_vma=False,
    )
```

profile of v0, /device:TPU:1, one launch (start us, length us, event | category | flops | bytes accessed | tf_op | source)
XLA Modules:
  0.0 322.6 jit_solution(17937538685821813687)
XLA Ops:
  7.2 0.0 all-gather.3.cloned.1.call-start
  7.2 0.9 copy.17
  8.1 0.2 eq.71
  8.3 0.2 eq.67
  8.5 0.7 broadcast_multiply_fusion.1
  9.2 9.0 %reduce-window.6 = s32[32,8,128]{2,1,0:T(8,128)S(1)} reduce-window(s32[32,8,128]{2,1,0:T(8,128)S(1)} %fusion.32, s32[]{:T(128)} %constant.81.clone.1), window={size=1x1x128 pad=0_0x0_0x127_0}, to_apply=%region_2.3 | reduce-window | flops 4161536 | bytes 262148 | tf_op jit(solution)/shard_map/reduce-window
  18.2 0.1 slice.102
  18.3 0.1 copy.19
  18.5 0.1 copy.20
  18.5 0.1 add_add_fusion
  18.7 0.1 copy.16
  18.8 0.2 mul.99
  19.1 4.3 %scatter_custom_fusion = s32[1536]{0:T(1024)S(1)} fusion(s32[1024]{0:T(1024)S(1)} %bitcast.63, s32[1024]{0:T(1024)S(1)} %fusion.33, s32[]{:T(128)} %constant.81.clone.1), kind=kCustom, calls=%fused_computation.76 | custom fusion | bytes 6148 | tf_op jit(solution)/shard_map/scatter | solution.py:114
  23.4 0.1 broadcast_in_dim.75
  23.5 3.6 %gather_fusion = bf16[1536,128]{1,0:T(8,128)(2,1)S(1)} fusion(bf16[512,128]{1,0:T(8,128)(2,1)} %param.13, s32[2048]{0:T(1024)S(1)} %pad_clamp_fusion), kind=kCustom, calls=%fused_computation | custom fusion | bytes 792576 | tf_op jit(solution)/shard_map/gather | solution.py:120
  27.1 0.3 broadcast_select_fusion
  27.4 44.4 %all_to_all.15 = bf16[32,48,128]{2,1,0:T(8,128)(2,1)} all-to-all(bf16[32,48,128]{2,1,0:T(8,128)(2,1)S(1)} %broadcast_select_fusion), channel_id=1, replica_groups=mesh['ep'=32,'tp'=16] {'ep'}, dimensions={0} | all-to-all | bytes 786432 | tf_op jit(solution)/shard_map/all_to_all | solution.py:121
  71.8 0.0 all-gather.3.cloned.1.call-update
  71.8 0.1 copy.15
  71.9 1.6 broadcast_in_dim.70
  73.5 6.9 %all-to-all-start = ((bf16[16,512,128]{1,2,0:T(8,128)(2,1)}), bf16[16,512,128]{1,2,0:T(8,128)(2,1)S(1)}, u32[]{:S(2)}, u32[]{:S(2)}) async-start(bf16[16,512,128]{1,2,0:T(8,128)(2,1)} %broadcast_in_dim.70), calls=%async_computation | async-start | bytes 4194304 | tf_op jit(solution)/shard_map/all_to_all | solution.py:36
  80.4 0.0 all-gather.5.cloned.1.call-start
  80.5 35.4 %all-to-all-done = bf16[16,512,128]{1,2,0:T(8,128)(2,1)S(1)} async-done(((bf16[16,512,128]{1,2,0:T(8,128)(2,1)}), bf16[16,512,128]{1,2,0:T(8,128)(2,1)S(1)}, u32[]{:S(2)}, u32[]{:S(2)}) %all-to-all-start) | async-done | bytes 2097184 | tf_op jit(solution)/shard_map/all_to_all | solution.py:36
  115.9 0.3 convert_reduce_fusion.1
  116.2 0.6 multiply_reduce_fusion
  116.9 0.6 fusion.9
  117.5 0.8 fusion.20
  118.3 1.9 collective-permute-start
  120.2 2.8 collective-permute-start.1
  123.1 2.0 collective-permute-done.1
  125.2 0.5 fusion.29
  125.7 30.2 %all-gather.3.cloned.1.call-done = bf16[1536,2048]{1,0:T(8,128)(2,1)} async-done(((bf16[1536,128]{1,0:T(8,128)(2,1)}), bf16[1536,2048]{1,0:T(8,128)(2,1)}) %all-gather.3.cloned.1.call-update) | async-done | bytes 6291472 | tf_op jit(solution)/shard_map/all_gather | solution.py:129
  155.9 3.8 %convert_reduce_fusion = f32[1536]{0:T(1024)S(1)} fusion(bf16[1536,2048]{1,0:T(8,128)(2,1)} %all-gather.3.cloned.1.call-done), kind=kLoop, calls=%fused_computation.4 | loop fusion | flops 6289920 | bytes 6297600 | tf_op jit(solution)/shard_map/reduce_sum | solution.py:56
  159.7 0.8 copy-done.1
  160.5 1.8 fusion.2
  162.3 2.4 fusion.4
  164.7 1.8 convolution_bitcast_fusion.1
  166.6 1.9 fusion.11
  168.5 0.9 pad_maximum_fusion
  169.3 0.0 all-gather.5.cloned.1.call-update
  169.4 92.1 %all-gather.5.cloned.1.call-done = bf16[2048,2048]{0,1:T(8,128)(2,1)} async-done(((bf16[128,2048]{0,1:T(8,128)(2,1)}), bf16[2048,2048]{0,1:T(8,128)(2,1)}) %all-gather.5.cloned.1.call-update) | async-done | bytes 8388624 | tf_op jit(solution)/shard_map/all_gather | solution.py:51
  261.5 5.4 %fusion.12 = bf16[1536,128]{1,0:T(8,128)(2,1)} fusion(bf16[2048,2048]{0,1:T(8,128)(2,1)} %all-gather.5.cloned.1.call-done, bf16[1,2048,128]{2,1,0:T(8,128)(2,1)S(1)} %copy-done.9), kind=kOutput, calls=%fused_computation.21 | convolution fusion | flops 805502976 | bytes 7208960 | tf_op jit(solution)/shard_map/dot_general | solution.py:149
  266.9 14.4 %all-to-all-start.2 = ((bf16[32,48,128]{2,1,0:T(8,128)(2,1)}), bf16[32,48,128]{2,1,0:T(8,128)(2,1)S(1)}, u32[]{:S(2)}, u32[]{:S(2)}) async-start(bf16[32,48,128]{2,1,0:T(8,128)(2,1)} %bitcast.14), calls=%async_computation.2 | async-start | bytes 786432 | tf_op jit(solution)/shard_map/all_to_all | solution.py:154
  281.3 0.1 copy.21
  281.5 3.0 fusion.17
  284.4 24.6 %all-to-all-done.2 = bf16[32,48,128]{2,1,0:T(8,128)(2,1)S(1)} async-done(((bf16[32,48,128]{2,1,0:T(8,128)(2,1)}), bf16[32,48,128]{2,1,0:T(8,128)(2,1)S(1)}, u32[]{:S(2)}, u32[]{:S(2)}) %all-to-all-start.2) | async-done | bytes 393248 | tf_op jit(solution)/shard_map/all_to_all | solution.py:154
  309.1 3.2 gather_fusion.1
  312.3 3.5 %fusion.21 = bf16[512,128]{1,0:T(8,128)(2,1)} fusion(bf16[512,2,128]{2,1,0:T(2,128)(2,1)S(1)} %bitcast.59, f32[512,2]{1,0:T(8,128)S(1)} %copy.21), kind=kLoop, calls=%fused_computation.30 | loop fusion | flops 327680 | bytes 397312 | tf_op jit(solution)/shard_map/reduce_sum | solution.py:158
  (42 shorter events, 0.3 us)
Async XLA Ops:
  7.2 157.6 %copy-start = (bf16[1,2048,128]{2,1,0:T(8,128)(2,1)S(1)}, bf16[1,2048,128]{2,1,0:T(8,128)(2,1)}, u32[]{:S(2)}) copy-start(bf16[1,2048,128]{2,1,0:T(8,128)(2,1)} %param.19) | copy-start | bytes 1572868
  7.2 64.6 %copy-start.3 = (bf16[512,128]{1,0:T(8,128)(2,1)S(1)}, bf16[512,128]{1,0:T(8,128)(2,1)}, u32[]{:S(2)}) copy-start(bf16[512,128]{1,0:T(8,128)(2,1)} %param.12) | copy-start | bytes 393220
  7.2 148.7 %all-gather.3.cloned.1.call-start = ((), (), s32[]{:S(2)}) async-start(), calls=%async_computation.3 | async-start | bytes 6684672 | tf_op jit(solution)/shard_map/all_gather | solution.py:129
  27.1 89.8 %copy-start.4 = (f32[2048]{0:T(1024)S(1)}, f32[2048]{0:T(1024)}, u32[]{:S(2)}) copy-start(f32[2048]{0:T(1024)} %param.14) | copy-start | bytes 24580
  73.5 44.0 %copy-start.2 = (bf16[2048,128]{1,0:T(8,128)(2,1)S(1)}, bf16[2048,128]{1,0:T(8,128)(2,1)}, u32[]{:S(2)}) copy-start(bf16[2048,128]{1,0:T(8,128)(2,1)} %param.16) | copy-start | bytes 1572868
  73.5 42.4 %all-to-all-start = ((bf16[16,512,128]{1,2,0:T(8,128)(2,1)}), bf16[16,512,128]{1,2,0:T(8,128)(2,1)S(1)}, u32[]{:S(2)}, u32[]{:S(2)}) async-start(bf16[16,512,128]{1,2,0:T(8,128)(2,1)} %broadcast_in_dim.70), calls=%async_computation | async-start | bytes 4194304 | tf_op jit(solution)/shard_map/all_to_all | solution.py:36
  80.4 44.8 %copy-start.7 = (f32[128]{0:T(128)S(1)}, f32[128]{0:T(128)}, u32[]{:S(2)}) copy-start(f32[128]{0:T(128)} %param.15) | copy-start | bytes 1540
  80.4 181.1 %all-gather.5.cloned.1.call-start = ((), (), s32[]{:S(2)}) async-start(), calls=%async_computation.4 | async-start | bytes 8912896 | tf_op jit(solution)/shard_map/all_gather | solution.py:51
  118.3 4.8 %collective-permute-start = (bf16[128,8]{0,1:T(8,128)(2,1)S(1)}, bf16[128,8]{0,1:T(8,128)(2,1)S(1)}, u32[]{:S(2)}, u32[]{:S(2)}) collective-permute-start(bf16[128,8]{0,1:T(8,128)(2,1)S(1)} %get-tuple-element.2), channel_id=1, source_target_pairs={{0,16},{16,32},{32,48},{48,64},{64,80},{80,96},{96,112},{112,128},... | collective-permute-start | bytes 6152 | tf_op jit(solution)/shard_map/ppermute | solution.py:20
  120.2 4.9 %collective-permute-start.1 = (bf16[128,8]{0,1:T(8,128)(2,1)S(1)}, bf16[128,8]{0,1:T(8,128)(2,1)S(1)}, u32[]{:S(2)}, u32[]{:S(2)}) collective-permute-start(bf16[128,8]{0,1:T(8,128)(2,1)S(1)} %get-tuple-element.3), channel_id=1, source_target_pairs={{16,0},{32,16},{48,32},{64,48},{80,64},{96,80},{112,96},{128,112},... | collective-permute-start | bytes 6152 | tf_op jit(solution)/shard_map/ppermute | solution.py:23
  125.7 36.6 %copy-start.5 = (f32[2048]{0:T(1024)S(1)}, f32[2048]{0:T(1024)}, u32[]{:S(2)}) copy-start(f32[2048]{0:T(1024)} %param.18) | copy-start | bytes 24580
  155.9 4.6 %copy-start.1 = (bf16[1536,2048]{1,0:T(8,128)(2,1)S(1)}, bf16[1536,2048]{1,0:T(8,128)(2,1)}, u32[]{:S(2)}) copy-start(bf16[1536,2048]{1,0:T(8,128)(2,1)} %all-gather.3.cloned.1.call-done) | copy-start | bytes 18874372
  164.7 1.9 copy-start.8
  166.6 94.9 %copy-start.9 = (bf16[1,2048,128]{2,1,0:T(8,128)(2,1)S(1)}, bf16[1,2048,128]{2,1,0:T(8,128)(2,1)}, u32[]{:S(2)}) copy-start(bf16[1,2048,128]{2,1,0:T(8,128)(2,1)} %param.21) | copy-start | bytes 1572868
  169.4 111.9 %copy-start.6 = (f32[512,2]{0,1:T(2,128)S(1)}, f32[512,2]{0,1:T(2,128)}, u32[]{:S(2)}) copy-start(f32[512,2]{0,1:T(2,128)} %param.23) | copy-start | bytes 12292
  169.4 112.1 %copy-start.10 = (bf16[2048,128]{1,0:T(8,128)(2,1)S(1)}, bf16[2048,128]{1,0:T(8,128)(2,1)}, u32[]{:S(2)}) copy-start(bf16[2048,128]{1,0:T(8,128)(2,1)} %param.17) | copy-start | bytes 1572868
  266.9 42.1 %all-to-all-start.2 = ((bf16[32,48,128]{2,1,0:T(8,128)(2,1)}), bf16[32,48,128]{2,1,0:T(8,128)(2,1)S(1)}, u32[]{:S(2)}, u32[]{:S(2)}) async-start(bf16[32,48,128]{2,1,0:T(8,128)(2,1)} %bitcast.14), calls=%async_computation.2 | async-start | bytes 786432 | tf_op jit(solution)/shard_map/all_to_all | solution.py:154
Sparse Core Ops, SparseCore 0:
  71.9 83.9 all-gather.2
  169.5 91.9 all-gather.4
where the time goes:
time: 323 us
  waiting for transfers between devices  184 us (57%)
  blocking collectives  44.4 us (14%)
  starting transfers between devices  26.1 us (8%)
  other arithmetic  24.8 us (8%)
  local copies, waits for them, and re-layouts  15.7 us (5%)
  between operations  14.4 us (4%)
  matrix products  12.8 us (4%)
    all_gather x1, waiting for transfers between devices, side_by_side(): lax.all_gather(both, axis, axis=dim, tiled=True)  92.1 us
    all_to_all x1, blocking collectives, on_device(): lax.all_to_all(outgoing.reshape(ep_size, capacity, feature_count), 'ep',...  44.4 us
    all_to_all x1, waiting for transfers between devices, sent_to_all(): lax.all_to_all(jnp.broadcast_to(array[None], (length, *array.shape)), axi...  35.4 us
    all_gather x1, waiting for transfers between devices, on_device(): lax.all_gather(slot_slices, 'tp', axis=1, tiled=True)  30.2 us
    all_to_all x1, waiting for transfers between devices, on_device(): lax.all_to_all(back_rows, 'ep', split_axis=0, concat_axis=0, tiled=True)  24.6 us
    all_to_all x1, starting transfers between devices, on_device(): lax.all_to_all(back_rows, 'ep', split_axis=0, concat_axis=0, tiled=True)  14.4 us
    another operation x2, other arithmetic  9.04 us
    all_to_all x1, starting transfers between devices, sent_to_all(): lax.all_to_all(jnp.broadcast_to(array[None], (length, *array.shape)), axi...  6.89 us
  transfers between devices with their start and end apart: 6, of which 5 were waited for; matrix products, arithmetic and copies ran while one was open for 2% of the time, Pallas kernels for 0%

commit v1 on v0

v1 whole, which is shorter than its diff:
```python
import jax
import jax.numpy as jnp
from jax import lax
from jax.experimental import pallas as pl
from jax.experimental.pallas import tpu as pltpu
from jax.sharding import PartitionSpec as P

MESH = pl.DeviceIdType.MESH
EPS = 1e-05
UNIT = 128
CAP = 48
SIDE = 4
M0, S0, P0, H0, UNITS = 0, 8, 20, 24, 36
LAG = 2
BF, F32 = jnp.bfloat16, jnp.float32


def kernel(
    mixer_ref,
    expert_ref,
    mgain_ref,
    scale_ref,
    egain_ref,
    routes_ref,
    routes_t_ref,
    rw_ref,
    w_in_hbm,
    w_mix_hbm,
    gate_hbm,
    up_hbm,
    down_hbm,
    mixer_out,
    expert_out,
    ring,
    w_in,
    w_mix,
    w_gu,
    w_down,
    outgoing,
    back,
    returned,
    normed,
    inner,
    halo,
    slot_of,
    picked,
    w_sem,
    send_sem,
    ring_sem,
    disp_send,
    disp_sem,
    back_send,
    back_sem,
    halo_send,
    halo_sem,
):
    ep, tp = lax.axis_index("ep"), lax.axis_index("tp")
    n_ep = lax.axis_size("ep")
    n_z = n_ep // 2
    rows = mixer_ref.shape[0]
    slots = n_ep * CAP
    z, core = ep // 2, ep % 2
    y, x = tp // SIDE, tp % SIDE
    yp, ym, xp, xm = (y + 1) % SIDE, (y + 3) % SIDE, (x + 1) % SIDE, (x + 3) % SIDE
    to_yp, to_ym = {"tp": yp * SIDE + x}, {"tp": ym * SIDE + x}
    to_xp, to_xm = {"tp": y * SIDE + xp}, {"tp": y * SIDE + xm}

    weights = [
        pltpu.make_async_copy(w_in_hbm, w_in, w_sem.at[0]),
        pltpu.make_async_copy(gate_hbm, w_gu.at[:, 0:128], w_sem.at[1]),
        pltpu.make_async_copy(up_hbm, w_gu.at[:, 128:256], w_sem.at[2]),
        pltpu.make_async_copy(w_mix_hbm, w_mix, w_sem.at[3]),
        pltpu.make_async_copy(down_hbm, w_down, w_sem.at[4]),
    ]
    for copy in weights:
        copy.start()

    barrier = pltpu.get_barrier_semaphore()

    def greet(j, carry):
        pl.semaphore_signal(
            barrier, inc=1, device_id={"ep": (ep + j) % n_ep}, device_id_type=MESH
        )
        return carry

    for peer in (to_yp, to_ym, to_xp, to_xm):
        pl.semaphore_signal(barrier, inc=1, device_id=peer, device_id_type=MESH)
    lax.fori_loop(1, n_ep, greet, 0)

    ring[y, x, 0:rows, :] = mixer_ref[...]

    half = n_z // 2

    def step_of(q):
        j = q // 2
        return jnp.where(j % 2 == 1, half - (j + 1) // 2, j // 2 - half)

    q_col = lax.broadcasted_iota(jnp.int32, (n_ep, 1), 0)
    q_row = lax.broadcasted_iota(jnp.int32, (1, n_ep), 1)

    def expert_at(q):
        other = (core + q % 2) % 2
        return (z + step_of(q) + n_z) % n_z * 2 + other

    e_col = expert_at(q_col)
    named = (routes_t_ref[0:1, :] == e_col) | (routes_t_ref[1:2, :] == e_col)
    r_iota = lax.broadcasted_iota(jnp.int32, (rows, rows), 0)
    c_iota = lax.broadcasted_iota(jnp.int32, (rows, rows), 1)
    before = jnp.where(r_iota < c_iota, 1.0, 0.0).astype(BF)
    rank = jnp.dot(
        jnp.where(named, 1.0, 0.0).astype(BF), before, preferred_element_type=F32
    )
    rank = jnp.where(named, rank, -1.0)
    place = lax.broadcasted_iota(jnp.int32, (CAP, rows), 0).astype(F32)
    for g in range(n_ep // 8):
        hot = jnp.concatenate(
            [
                jnp.where(rank[q : q + 1, :] == place, 1.0, 0.0).astype(BF)
                for q in range(8 * g, 8 * g + 8)
            ],
            axis=0,
        )
        outgoing[8 * CAP * g : 8 * CAP * (g + 1), :] = jnp.dot(
            hot, expert_ref[...], preferred_element_type=F32
        ).astype(BF)
    own = (n_ep - 2) * CAP
    ring[y, x, S0 * UNIT + own : S0 * UNIT + own + CAP, :] = outgoing[own : own + CAP, :]

    pl.semaphore_wait(barrier, n_ep - 1 + 4)

    def remote(src, dst, send, recv, device):
        pltpu.make_async_remote_copy(
            src_ref=src,
            dst_ref=dst,
            send_sem=send,
            recv_sem=recv,
            device_id=device,
            device_id_type=MESH,
        ).start()

    def await_bytes(ref, sem):
        pltpu.make_async_copy(ref, ref, sem).wait()

    def ring_copy(ref, sem, device):
        remote(ref, ref, send_sem, sem, device)

    def first_a(u):
        r = u * UNIT
        lo, hi = pl.ds(r, 64), pl.ds(r + 64, 64)
        ring_copy(ring.at[y, x, lo], ring_sem.at[u, 0, 0], to_xp)
        ring_copy(ring.at[y, x, hi], ring_sem.at[u, 1, 0], to_yp)
        ring_copy(ring.at[y, x, lo], ring_sem.at[u, 0, 0], to_xm)
        ring_copy(ring.at[y, x, hi], ring_sem.at[u, 1, 0], to_ym)

    def second_a(u):
        r = u * UNIT
        await_bytes(ring.at[y, x, pl.ds(r, 128)], ring_sem.at[u, 0, 0])
        await_bytes(ring.at[y, x, pl.ds(r, 128)], ring_sem.at[u, 1, 0])
        ring_copy(ring.at[y, xm, pl.ds(r, 32)], ring_sem.at[u, 0, 1], to_xp)
        ring_copy(ring.at[ym, x, pl.ds(r + 64, 32)], ring_sem.at[u, 1, 1], to_yp)
        ring_copy(ring.at[y, xp, pl.ds(r + 32, 32)], ring_sem.at[u, 0, 1], to_xm)
        ring_copy(ring.at[yp, x, pl.ds(r + 96, 32)], ring_sem.at[u, 1, 1], to_ym)

    def first_b(u):
        r = u * UNIT
        lo, hi = pl.ds(r, 64), pl.ds(r + 64, 64)
        await_bytes(ring.at[y, x, lo], ring_sem.at[u, 0, 1])
        await_bytes(ring.at[y, x, lo], ring_sem.at[u, 1, 1])
        ring_copy(ring.at[y, :, lo], ring_sem.at[u, 0, 2], to_yp)
        ring_copy(ring.at[:, x, hi], ring_sem.at[u, 1, 2], to_xp)
        ring_copy(ring.at[y, :, lo], ring_sem.at[u, 0, 2], to_ym)
        ring_copy(ring.at[:, x, hi], ring_sem.at[u, 1, 2], to_xm)

    def second_b(u):
        r = u * UNIT
        await_bytes(ring.at[y, :, pl.ds(r, 128)], ring_sem.at[u, 0, 2])
        await_bytes(ring.at[y, :, pl.ds(r, 128)], ring_sem.at[u, 1, 2])
        ring_copy(ring.at[ym, :, pl.ds(r, 32)], ring_sem.at[u, 0, 3], to_yp)
        ring_copy(ring.at[:, xm, pl.ds(r + 64, 32)], ring_sem.at[u, 1, 3], to_xp)
        ring_copy(ring.at[yp, :, pl.ds(r + 32, 32)], ring_sem.at[u, 0, 3], to_ym)
        ring_copy(ring.at[:, xp, pl.ds(r + 96, 32)], ring_sem.at[u, 1, 3], to_xm)

    def finished(u):
        r = u * UNIT
        await_bytes(ring.at[y, :, pl.ds(r, 64)], ring_sem.at[u, 0, 3])
        await_bytes(ring.at[y, :, pl.ds(r, 64)], ring_sem.at[u, 1, 3])

    def peer_at(q, sign):
        dz = half - (q // 2 + 1) // 2 if (q // 2) % 2 == 1 else q // 2 // 2 - half
        other = (core + q % 2) % 2
        return {"ep": (z + sign * dz + n_z) % n_z * 2 + other}

    for q in range(n_ep):
        if q != n_ep - 2:
            remote(
                outgoing.at[q * CAP : (q + 1) * CAP],
                ring.at[y, x, S0 * UNIT + q * CAP : S0 * UNIT + (q + 1) * CAP],
                disp_send,
                disp_sem.at[q // 8],
                peer_at(q, 1),
            )

    e_row = expert_at(q_row)
    hits = [routes_ref[:, k : k + 1] == e_row for k in range(2)]
    after = jnp.where(c_iota < r_iota, 1.0, 0.0).astype(BF)
    rank_c = jnp.dot(
        after, jnp.where(hits[0] | hits[1], 1.0, 0.0).astype(BF), preferred_element_type=F32
    )
    base = q_row.astype(F32) * float(CAP)
    for k in range(2):
        at = jnp.sum(jnp.where(hits[k], rank_c + base, 0.0), axis=1, keepdims=True)
        slot_of[k * rows : (k + 1) * rows, :] = jnp.broadcast_to(at, (rows, 128))
    picked[...] = jnp.zeros_like(picked)

    def layer_norm(u, gain_ref):
        def block(b, carry):
            r = pl.ds(u * UNIT + b * 32, 32)

            def piece(p):
                return ring[p // SIDE, p % SIDE, r, :].astype(F32)

            n = SIDE * SIDE
            total = piece(0)
            for p in range(1, n):
                total = total + piece(p)
            mean = jnp.sum(total, axis=1, keepdims=True) * (1.0 / (n * 128))
            square = None
            for p in range(n):
                d = piece(p) - mean
                square = d * d if square is None else square + d * d
            var = jnp.sum(square, axis=1, keepdims=True) * (1.0 / (n * 128))
            inv = lax.rsqrt(var + EPS)
            for p in range(n):
                normed[pl.ds(b * 32, 32), p * 128 : (p + 1) * 128] = (
                    (piece(p) - mean) * inv * gain_ref[p : p + 1, :]
                ).astype(BF)
            return carry

        lax.fori_loop(0, UNIT // 32, block, 0)

    def wide(u):
        r = pl.ds(u * UNIT, UNIT)
        return jnp.concatenate(
            [ring[p // SIDE, p % SIDE, r, :] for p in range(SIDE * SIDE)], axis=1
        )

    def mixer_unit(u):
        layer_norm(u, mgain_ref)
        inner[pl.ds((u - M0) * UNIT, UNIT), :] = jnp.dot(
            normed[...], w_in[...], preferred_element_type=F32
        ).astype(BF)

    def slot_unit(u):
        layer_norm(u, egain_ref)
        both = jnp.dot(normed[...], w_gu[...], preferred_element_type=F32)
        gate, up = both[:, 0:128], both[:, 128:256]
        hidden = gate / (1.0 + jnp.exp(-gate)) * up
        ring[y, x, pl.ds((u - S0 + H0) * UNIT, UNIT), :] = hidden.astype(BF)

    def pooled_unit(u):
        mixer_out[pl.ds((u - P0) * UNIT, UNIT), :] = jnp.dot(
            wide(u), w_mix[...], preferred_element_type=F32
        ).astype(BF)

    def hidden_unit(u):
        back[pl.ds((u - H0) * UNIT, UNIT), :] = jnp.dot(
            wide(u), w_down[...], preferred_element_type=F32
        ).astype(BF)

    def halo_out():
        remote(
            inner.at[rows - 16 : rows],
            halo.at[0:16],
            halo_send,
            halo_sem.at[0],
            {"ep": (ep + 1) % n_ep},
        )
        remote(
            inner.at[0:16],
            halo.at[16:32],
            halo_send,
            halo_sem.at[1],
            {"ep": (ep + n_ep - 1) % n_ep},
        )

    def pool():
        await_bytes(halo.at[0:16], halo_sem.at[0])
        await_bytes(halo.at[16:32], halo_sem.at[1])
        low = jnp.where(ep > 0, halo[8:16, :].astype(F32), 0.0)
        high = jnp.where(ep < n_ep - 1, halo[16:24, :].astype(F32), 0.0)
        values = inner[...].astype(F32)
        ext = jnp.concatenate([low, values, high], axis=0)
        two = ext[0 : rows + 15, :] + ext[1 : rows + 16, :]
        four = two[0 : rows + 13, :] + two[2 : rows + 15, :]
        eight = four[0 : rows + 9, :] + four[4 : rows + 13, :]
        sixteen = eight[0 : rows + 1, :] + eight[8 : rows + 9, :]
        total = jnp.where(
            y == 0,
            two[7 : 7 + rows, :],
            jnp.where(
                y == 1,
                four[6 : 6 + rows, :],
                jnp.where(y == 2, eight[4 : 4 + rows, :], sixteen[0:rows, :]),
            ),
        )
        reach = jnp.where(y == 0, 1, jnp.where(y == 1, 2, jnp.where(y == 2, 4, 8)))
        token = ep * rows + lax.broadcasted_iota(jnp.int32, (rows, 128), 0)
        count = jnp.minimum(token + reach, n_ep * rows) - jnp.maximum(token - reach, 0)
        result = (total / count.astype(F32) - values) * scale_ref[...]
        ring[y, x, P0 * UNIT : P0 * UNIT + rows, :] = result.astype(BF)

    def send_back(g):
        for q in range(8 * g, 8 * g + 8):
            part = slice(q * CAP, (q + 1) * CAP)
            if q == n_ep - 2:
                returned[part, :] = back[part, :]
            else:
                remote(
                    back.at[part], returned.at[part], back_send, back_sem.at[g], peer_at(q, -1)
                )

    group = 8 * CAP
    lane = lax.broadcasted_iota(jnp.int32, (2 * rows, 128), 1).astype(F32)

    def combine(g):
        count = group if 8 * g + 8 < n_ep else group - CAP
        await_bytes(returned.at[0:count], back_sem.at[g])
        where = slot_of[...]
        hot = jnp.concatenate(
            [
                jnp.where(where == lane + float(g * group + c * 128), 1.0, 0.0).astype(BF)
                for c in range(group // 128)
            ],
            axis=1,
        )
        picked[...] += jnp.dot(
            hot, returned[g * group : (g + 1) * group, :], preferred_element_type=F32
        )

    n_groups = n_ep // 8

    def sends(u):
        return ((u >= M0) & (u < M0 + rows // UNIT)) | ((u >= S0) & (u < UNITS))

    def step(i, carry):
        for lag, stage in ((3 * LAG, second_b), (2 * LAG, first_b), (LAG, second_a)):
            u = i - lag

            @pl.when(sends(u))
            def _():
                stage(u)

        for g in range(n_groups):

            @pl.when(i == S0 + 3 * g)
            def _():
                count = group if g + 1 < n_groups else group - CAP
                await_bytes(ring.at[y, x, 0:count], disp_sem.at[g])

        @pl.when(sends(i))
        def _():
            first_a(i)

        u = i - 4 * LAG

        @pl.when(sends(u))
        def _():
            finished(u)

        @pl.when(u == M0)
        def _():
            for copy in weights:
                copy.wait()

        @pl.when((u >= M0) & (u < M0 + rows // UNIT))
        def _():
            mixer_unit(u)

        @pl.when(u == M0 + rows // UNIT - 1)
        def _():
            halo_out()

        @pl.when(u == M0 + rows // UNIT + 2)
        def _():
            pool()

        @pl.when((u >= S0) & (u < P0))
        def _():
            slot_unit(u)

        @pl.when((u >= P0) & (u < H0))
        def _():
            pooled_unit(u)

        @pl.when(u >= H0)
        def _():
            hidden_unit(u)

        for g in range(n_groups):

            @pl.when(u == H0 + 3 * g + 2)
            def _():
                if g > 0:
                    combine(g - 1)
                send_back(g)

        return carry

    lax.fori_loop(0, UNITS + 4 * LAG, step, 0)
    combine(n_groups - 1)
    expert_out[...] = (
        picked[0:rows, :] * rw_ref[:, 0:1] + picked[rows : 2 * rows, :] * rw_ref[:, 1:2]
    ).astype(BF)
    sent = (SIDE * SIDE - 1) * (2 * rows + 2 * slots) // (SIDE * SIDE)
    await_bytes(ring.at[:, :, 0:sent], send_sem)
    await_bytes(outgoing.at[0 : slots - CAP], disp_send)
    await_bytes(back.at[0 : slots - CAP], back_send)
    await_bytes(inner.at[0:32], halo_send)


def on_device(
    mixer_rows,
    expert_rows,
    mixer_gain,
    pool_scale,
    w_in,
    w_mix_out,
    expert_gain,
    expert_gate,
    expert_up,
    expert_down,
    routes,
    route_weight,
):
    rows, feats = mixer_rows.shape
    n_ep = lax.axis_size("ep")
    depth = w_in.shape[0]
    vmem = pl.BlockSpec(memory_space=pltpu.VMEM)
    hbm = pl.BlockSpec(memory_space=pl.ANY)
    slots = n_ep * CAP
    return pl.pallas_call(
        kernel,
        name="mixer_and_experts",
        out_shape=(
            jax.ShapeDtypeStruct((rows, feats), BF),
            jax.ShapeDtypeStruct((rows, feats), BF),
        ),
        in_specs=[vmem] * 8 + [hbm] * 5,
        out_specs=(vmem, vmem),
        scratch_shapes=[
            pltpu.VMEM((SIDE, SIDE, UNITS * UNIT, feats), BF),
            pltpu.VMEM((depth, 128), BF),
            pltpu.VMEM((depth, 128), BF),
            pltpu.VMEM((depth, 256), BF),
            pltpu.VMEM((depth, 128), BF),
            pltpu.VMEM((slots, feats), BF),
            pltpu.VMEM((slots, feats), BF),
            pltpu.VMEM((slots, feats), BF),
            pltpu.VMEM((UNIT, depth), BF),
            pltpu.VMEM((rows, feats), BF),
            pltpu.VMEM((32, feats), BF),
            pltpu.VMEM((2 * rows, 128), F32),
            pltpu.VMEM((2 * rows, feats), F32),
            pltpu.SemaphoreType.DMA((5,)),
            pltpu.SemaphoreType.DMA,
            pltpu.SemaphoreType.DMA((UNITS, 2, 4)),
            pltpu.SemaphoreType.DMA,
            pltpu.SemaphoreType.DMA((n_ep // 8,)),
            pltpu.SemaphoreType.DMA,
            pltpu.SemaphoreType.DMA((n_ep // 8,)),
            pltpu.SemaphoreType.DMA,
            pltpu.SemaphoreType.DMA((2,)),
        ],
        compiler_params=pltpu.CompilerParams(
            collective_id=0, has_side_effects=True, vmem_limit_bytes=60 * 1024 * 1024
        ),
    )(
        mixer_rows,
        expert_rows,
        mixer_gain.reshape(-1, 128),
        pool_scale.reshape(1, -1),
        expert_gain.reshape(-1, 128),
        routes,
        routes.T,
        route_weight,
        w_in,
        w_mix_out,
        expert_gate[0],
        expert_up[0],
        expert_down[0],
    )


def solution(mesh):
    return jax.shard_map(
        on_device,
        mesh=mesh,
        in_specs=(
            P("ep", "tp"),
            P("ep", "tp"),
            P(),
            P("tp"),
            P(None, "tp"),
            P(None, "tp"),
            P(),
            P("ep", None, "tp"),
            P("ep", None, "tp"),
            P("ep", None, "tp"),
            P("ep", None),
            P("ep", None),
        ),
        out_specs=(P("ep", "tp"), P("ep", "tp")),
        check_vma=False,
    )
```

time: 323 us -> 138 us (0.43)
  waiting for transfers between devices: 184 us -> 0 us
  Pallas kernels: 0 us -> 133 us
  blocking collectives: 44.4 us -> 0 us
  starting transfers between devices: 26.1 us -> 0 us
  other arithmetic: 24.8 us -> 0 us
  between operations: 14.4 us -> 0.66 us
  matrix products: 12.8 us -> 0 us
  local copies, waits for them, and re-layouts: 15.7 us -> 4.64 us
    pallas_call x0 -> x1, Pallas kernels: none -> 133 us  [on_device(): pl.pallas_call(kernel, name='mixer_and_experts', out_shape=(jax.ShapeDtyp...]
    all_gather x2 -> x0, waiting for transfers between devices: 122 us -> none  [the longest x1 92.1 us: side_by_side(): lax.all_gather(both, axis, axis=dim, tiled=True)]
    all_to_all x2 -> x0, waiting for transfers between devices: 60 us -> none  [the longest x1 35.4 us: sent_to_all(): lax.all_to_all(jnp.broadcast_to(array[None], (length, *array.shape)), axi...]
    all_to_all x1 -> x0, blocking collectives: 44.4 us -> none  [on_device(): lax.all_to_all(outgoing.reshape(ep_size, capacity, feature_count), 'ep',...]
    all_to_all x2 -> x0, starting transfers between devices: 21.3 us -> none  [the longest x1 14.4 us: on_device(): lax.all_to_all(back_rows, 'ep', split_axis=0, concat_axis=0, tiled=True)]
    dot_general x5 -> x0, matrix products: 12.8 us -> none  [the longest x1 5.4 us: on_device(): lax.dot_general(pieces[1], down_weight, contract_lead, preferred_element_...]
    reduce_sum x6 -> x0, other arithmetic: 10.1 us -> none  [the longest x2 4.17 us: layer_norm(): center = values - jnp.mean(values, axis=-1, keepdims=True)]
    another operation x2 -> x0, other arithmetic: 9.04 us -> none
  transfers between devices with their start and end apart: 6 -> 0, of which waited for: 5 -> 0; matrix products, arithmetic and copies ran while one was open for 2% -> 0% of each run, Pallas kernels for 0% -> 0%
where the time goes in v1:
time: 138 us
  Pallas kernels  133 us (96%)
  local copies, waits for them, and re-layouts  4.64 us (3%)
    pallas_call x1, Pallas kernels, on_device(): pl.pallas_call(kernel, name='mixer_and_experts', out_shape=(jax.ShapeDtyp...  133 us
    unnamed x10, local copies, waits for them, and re-layouts  4.64 us

profile of v1, /device:TPU:1, one launch (start us, length us, event | category | flops | bytes accessed | tf_op | source)
XLA Modules:
  0.0 138.0 jit_solution(17132451993528047342)
XLA Ops:
  0.6 0.0 copy-start.2
  0.6 0.7 copy-done.2
  1.3 0.0 copy-start.1
  1.3 0.8 copy.15.rw_ref
  2.2 0.0 copy-done.1
  2.2 0.8 copy.14.routes_ref
  3.0 132.7 %mixer_and_experts.1 = (bf16[512,128]{1,0:T(8,128)(2,1)}, bf16[512,128]{1,0:T(8,128)(2,1)}) custom-call(bf16[512,128]{1,0:T(8,128)(2,1)} %mixer_ref.1, bf16[512,128]{1,0:T(8,128)(2,1)} %expert_ref.1, f32[16,128]{1,0:T(8,128)} %bitcast.11, f32[1,128]{1,0:T(1,128)} %bitcast.13, f32[16,128]{1,0:T(8,128)} %bitcast.12, s32[512,2]{1,0:T(8,128)} %copy.14.routes_ref, ...), custom_call_target="tpu_custom_call" | custom-call | tf_op jit(solution)/shard_map/mixer_and_experts/pallas_call | solution.py:441
  135.7 0.0 copy-start
  135.8 1.6 %copy.18 = bf16[512,128]{1,0:T(8,128)(2,1)} copy(bf16[512,128]{1,0:T(8,128)(2,1)} %get-tuple-element.4) | data formatting | bytes 262144
  137.4 0.0 copy-done
  137.4 0.7 copy.19
Async XLA Ops:
  0.6 0.7 copy-start.2
  1.3 0.9 copy-start.1
  135.7 1.6 %copy-start = (bf16[512,128]{1,0:T(8,128)(2,1)S(1)}, bf16[512,128]{1,0:T(8,128)(2,1)}, u32[]{:S(2)}) copy-start(bf16[512,128]{1,0:T(8,128)(2,1)} %get-tuple-element.5) | copy-start | bytes 393220

commit v2 on v1

--- a/solution.py
+++ b/solution.py
@@ -10,7 +10,7 @@
 UNIT = 128
 CAP = 48
 SIDE = 4
-M0, S0, P0, H0, UNITS = 0, 8, 20, 24, 36
+M0, S0, H0, P0, UNITS = 0, 4, 16, 28, 32
 LAG = 2
 BF, F32 = jnp.bfloat16, jnp.float32
 
@@ -21,9 +21,8 @@
     mgain_ref,
     scale_ref,
     egain_ref,
-    routes_ref,
     routes_t_ref,
-    rw_ref,
+    rw_t_ref,
     w_in_hbm,
     w_mix_hbm,
     gate_hbm,
@@ -43,6 +42,8 @@
     inner,
     halo,
     slot_of,
+    weight_of,
+    ranks,
     picked,
     w_sem,
     send_sem,
@@ -89,14 +90,11 @@
 
     ring[y, x, 0:rows, :] = mixer_ref[...]
 
-    half = n_z // 2
-
     def step_of(q):
         j = q // 2
-        return jnp.where(j % 2 == 1, half - (j + 1) // 2, j // 2 - half)
+        return jnp.where(j % 2 == 1, (j + 1) // 2, 0 - j // 2)
 
     q_col = lax.broadcasted_iota(jnp.int32, (n_ep, 1), 0)
-    q_row = lax.broadcasted_iota(jnp.int32, (1, n_ep), 1)
 
     def expert_at(q):
         other = (core + q % 2) % 2
@@ -111,6 +109,7 @@
         jnp.where(named, 1.0, 0.0).astype(BF), before, preferred_element_type=F32
     )
     rank = jnp.where(named, rank, -1.0)
+    ranks[...] = rank
     place = lax.broadcasted_iota(jnp.int32, (CAP, rows), 0).astype(F32)
     for g in range(n_ep // 8):
         hot = jnp.concatenate(
@@ -123,8 +122,7 @@
         outgoing[8 * CAP * g : 8 * CAP * (g + 1), :] = jnp.dot(
             hot, expert_ref[...], preferred_element_type=F32
         ).astype(BF)
-    own = (n_ep - 2) * CAP
-    ring[y, x, S0 * UNIT + own : S0 * UNIT + own + CAP, :] = outgoing[own : own + CAP, :]
+    ring[y, x, S0 * UNIT : S0 * UNIT + CAP, :] = outgoing[0:CAP, :]
 
     pl.semaphore_wait(barrier, n_ep - 1 + 4)
 
@@ -186,30 +184,31 @@
         await_bytes(ring.at[y, :, pl.ds(r, 64)], ring_sem.at[u, 1, 3])
 
     def peer_at(q, sign):
-        dz = half - (q // 2 + 1) // 2 if (q // 2) % 2 == 1 else q // 2 // 2 - half
+        dz = (q // 2 + 1) // 2 if (q // 2) % 2 == 1 else -(q // 2 // 2)
         other = (core + q % 2) % 2
         return {"ep": (z + sign * dz + n_z) % n_z * 2 + other}
 
-    for q in range(n_ep):
-        if q != n_ep - 2:
-            remote(
-                outgoing.at[q * CAP : (q + 1) * CAP],
-                ring.at[y, x, S0 * UNIT + q * CAP : S0 * UNIT + (q + 1) * CAP],
-                disp_send,
-                disp_sem.at[q // 8],
-                peer_at(q, 1),
-            )
-
-    e_row = expert_at(q_row)
-    hits = [routes_ref[:, k : k + 1] == e_row for k in range(2)]
-    after = jnp.where(c_iota < r_iota, 1.0, 0.0).astype(BF)
-    rank_c = jnp.dot(
-        after, jnp.where(hits[0] | hits[1], 1.0, 0.0).astype(BF), preferred_element_type=F32
-    )
-    base = q_row.astype(F32) * float(CAP)
-    for k in range(2):
-        at = jnp.sum(jnp.where(hits[k], rank_c + base, 0.0), axis=1, keepdims=True)
-        slot_of[k * rows : (k + 1) * rows, :] = jnp.broadcast_to(at, (rows, 128))
+    for u in range(M0, M0 + rows // UNIT):
+        first_a(u)
+    for q in range(1, n_ep):
+        remote(
+            outgoing.at[q * CAP : (q + 1) * CAP],
+            ring.at[y, x, S0 * UNIT + q * CAP : S0 * UNIT + (q + 1) * CAP],
+            disp_send,
+            disp_sem.at[q // 8],
+            peer_at(q, 1),
+        )
+
+    def place_results():
+        e_at = expert_at(q_col)
+        base = q_col.astype(F32) * float(CAP)
+        for k in range(2):
+            mine = routes_t_ref[k : k + 1, :] == e_at
+            at = jnp.sum(jnp.where(mine, ranks[...] + base, 0.0), axis=0, keepdims=True)
+            part = slice(k * rows, (k + 1) * rows)
+            slot_of[part, :] = jnp.broadcast_to(at, (128, rows)).T
+            weight_of[part, :] = jnp.broadcast_to(rw_t_ref[k : k + 1, :], (128, rows)).T
+
     picked[...] = jnp.zeros_like(picked)
 
     def layer_norm(u, gain_ref):
@@ -312,7 +311,7 @@
     def send_back(g):
         for q in range(8 * g, 8 * g + 8):
             part = slice(q * CAP, (q + 1) * CAP)
-            if q == n_ep - 2:
+            if q == 0:
                 returned[part, :] = back[part, :]
             else:
                 remote(
@@ -323,7 +322,7 @@
     lane = lax.broadcasted_iota(jnp.int32, (2 * rows, 128), 1).astype(F32)
 
     def combine(g):
-        count = group if 8 * g + 8 < n_ep else group - CAP
+        count = group if g > 0 else group - CAP
         await_bytes(returned.at[0:count], back_sem.at[g])
         where = slot_of[...]
         hot = jnp.concatenate(
@@ -354,14 +353,26 @@
 
             @pl.when(i == S0 + 3 * g)
             def _():
-                count = group if g + 1 < n_groups else group - CAP
+                count = group if g > 0 else group - CAP
                 await_bytes(ring.at[y, x, 0:count], disp_sem.at[g])
 
-        @pl.when(sends(i))
+        @pl.when((i >= S0) & (i < UNITS))
         def _():
             first_a(i)
 
+        @pl.when(i == S0 + 4)
+        def _():
+            place_results()
+
         u = i - 4 * LAG
+
+        @pl.when(u == UNITS - 1)
+        def _():
+            combine(n_groups - 1)
+            expert_out[...] = (
+                picked[0:rows, :] * weight_of[0:rows, :]
+                + picked[rows : 2 * rows, :] * weight_of[rows : 2 * rows, :]
+            ).astype(BF)
 
         @pl.when(sends(u))
         def _():
@@ -384,15 +395,15 @@
         def _():
             pool()
 
-        @pl.when((u >= S0) & (u < P0))
+        @pl.when((u >= S0) & (u < H0))
         def _():
             slot_unit(u)
 
-        @pl.when((u >= P0) & (u < H0))
+        @pl.when(u >= P0)
         def _():
             pooled_unit(u)
 
-        @pl.when(u >= H0)
+        @pl.when((u >= H0) & (u < P0))
         def _():
             hidden_unit(u)
 
@@ -407,10 +418,6 @@
         return carry
 
     lax.fori_loop(0, UNITS + 4 * LAG, step, 0)
-    combine(n_groups - 1)
-    expert_out[...] = (
-        picked[0:rows, :] * rw_ref[:, 0:1] + picked[rows : 2 * rows, :] * rw_ref[:, 1:2]
-    ).astype(BF)
     sent = (SIDE * SIDE - 1) * (2 * rows + 2 * slots) // (SIDE * SIDE)
     await_bytes(ring.at[:, :, 0:sent], send_sem)
     await_bytes(outgoing.at[0 : slots - CAP], disp_send)
@@ -445,7 +452,7 @@
             jax.ShapeDtypeStruct((rows, feats), BF),
             jax.ShapeDtypeStruct((rows, feats), BF),
         ),
-        in_specs=[vmem] * 8 + [hbm] * 5,
+        in_specs=[vmem] * 7 + [hbm] * 5,
         out_specs=(vmem, vmem),
         scratch_shapes=[
             pltpu.VMEM((SIDE, SIDE, UNITS * UNIT, feats), BF),
@@ -460,6 +467,8 @@
             pltpu.VMEM((rows, feats), BF),
             pltpu.VMEM((32, feats), BF),
             pltpu.VMEM((2 * rows, 128), F32),
+            pltpu.VMEM((2 * rows, 128), F32),
+            pltpu.VMEM((n_ep, rows), F32),
             pltpu.VMEM((2 * rows, feats), F32),
             pltpu.SemaphoreType.DMA((5,)),
             pltpu.SemaphoreType.DMA,
@@ -480,9 +489,8 @@
         mixer_gain.reshape(-1, 128),
         pool_scale.reshape(1, -1),
         expert_gain.reshape(-1, 128),
-        routes,
         routes.T,
-        route_weight,
+        route_weight.T,
         w_in,
         w_mix_out,
         expert_gate[0],

time: 138 us -> 125 us (0.906)
  Pallas kernels: 133 us -> 122 us
  local copies, waits for them, and re-layouts: 4.64 us -> 2.26 us
    pallas_call x1, Pallas kernels: 133 us -> 122 us  [on_device(): pl.pallas_call(kernel, name='mixer_and_experts', out_shape=(jax.ShapeDtyp...]
    unnamed x10 -> x4, local copies, waits for them, and re-layouts: 4.64 us -> 2.26 us
where the time goes in v2:
time: 125 us
  Pallas kernels  122 us (98%)
  local copies, waits for them, and re-layouts  2.26 us (2%)
    pallas_call x1, Pallas kernels, on_device(): pl.pallas_call(kernel, name='mixer_and_experts', out_shape=(jax.ShapeDtyp...  122 us

profile of v2, /device:TPU:1, one launch (start us, length us, event | category | flops | bytes accessed | tf_op | source)
XLA Modules:
  0.0 124.6 jit_solution(11053713379675888669)
XLA Ops:
  0.6 121.7 %mixer_and_experts.1 = (bf16[512,128]{1,0:T(8,128)(2,1)}, bf16[512,128]{1,0:T(8,128)(2,1)}) custom-call(bf16[512,128]{1,0:T(8,128)(2,1)} %mixer_ref.1, bf16[512,128]{1,0:T(8,128)(2,1)} %expert_ref.1, f32[16,128]{1,0:T(8,128)} %bitcast.11, f32[1,128]{1,0:T(1,128)} %bitcast.15, f32[16,128]{1,0:T(8,128)} %bitcast.12, s32[2,512]{1,0:T(2,128)} %bitcast.13, ...), custom_call_target="tpu_custom_call" | custom-call | tf_op jit(solution)/shard_map/mixer_and_experts/pallas_call | solution.py:448
  122.4 0.0 copy-start
  122.4 1.6 %copy.16 = bf16[512,128]{1,0:T(8,128)(2,1)} copy(bf16[512,128]{1,0:T(8,128)(2,1)} %get-tuple-element.4) | data formatting | bytes 262144
  124.0 0.0 copy-done
  124.0 0.7 copy.17
Async XLA Ops:
  122.4 1.6 %copy-start = (bf16[512,128]{1,0:T(8,128)(2,1)S(1)}, bf16[512,128]{1,0:T(8,128)(2,1)}, u32[]{:S(2)}) copy-start(bf16[512,128]{1,0:T(8,128)(2,1)} %get-tuple-element.5) | copy-start | bytes 393220

commit v3 on v2

--- a/solution.py
+++ b/solution.py
@@ -8,28 +8,28 @@
 MESH = pl.DeviceIdType.MESH
 EPS = 1e-05
 UNIT = 128
+SLOT_UNITS, TURN = 12, 3
 CAP = 48
 SIDE = 4
 M0, S0, H0, P0, UNITS = 0, 4, 16, 28, 32
-LAG = 2
+A2, B1, B2, DONE = 2, 4, 6, 8
 BF, F32 = jnp.bfloat16, jnp.float32
 
 
 def kernel(
-    mixer_ref,
-    expert_ref,
-    mgain_ref,
-    scale_ref,
-    egain_ref,
-    routes_t_ref,
-    rw_t_ref,
+    mixer_hbm,
+    expert_hbm,
+    mgain_hbm,
+    scale_hbm,
+    egain_hbm,
+    routes_t_hbm,
+    rw_t_hbm,
     w_in_hbm,
     w_mix_hbm,
     gate_hbm,
     up_hbm,
     down_hbm,
-    mixer_out,
-    expert_out,
+    out,
     ring,
     w_in,
     w_mix,
@@ -45,7 +45,14 @@
     weight_of,
     ranks,
     picked,
+    expert_ref,
+    mgain_ref,
+    scale_ref,
+    egain_ref,
+    routes_t_ref,
+    rw_t_ref,
     w_sem,
+    in_sem,
     send_sem,
     ring_sem,
     disp_send,
@@ -58,7 +65,7 @@
     ep, tp = lax.axis_index("ep"), lax.axis_index("tp")
     n_ep = lax.axis_size("ep")
     n_z = n_ep // 2
-    rows = mixer_ref.shape[0]
+    rows = mixer_hbm.shape[0]
     slots = n_ep * CAP
     z, core = ep // 2, ep % 2
     y, x = tp // SIDE, tp % SIDE
@@ -66,29 +73,41 @@
     to_yp, to_ym = {"tp": yp * SIDE + x}, {"tp": ym * SIDE + x}
     to_xp, to_xm = {"tp": y * SIDE + xp}, {"tp": y * SIDE + xm}
 
-    weights = [
+    barrier = pltpu.get_barrier_semaphore()
+
+    def peer_at(q, sign):
+        dz = (q // 2 + 1) // 2 if (q // 2) % 2 == 1 else -(q // 2 // 2)
+        other = (core + q % 2) % 2
+        return {"ep": (z + sign * dz + n_z) % n_z * 2 + other}
+
+    across_y, across_x = {"tp": (y + 2) % SIDE * SIDE + x}, {"tp": y * SIDE + (x + 2) % SIDE}
+    plane = (to_yp, to_ym, to_xp, to_xm, across_y, across_x)
+    for peer in [peer_at(q, 1) for q in range(n_ep - 1, 0, -1)] + list(plane):
+        pl.semaphore_signal(barrier, inc=1, device_id=peer, device_id_type=MESH)
+
+    own_rows = pltpu.make_async_copy(mixer_hbm, ring.at[y, x, 0:rows], in_sem.at[0])
+    inputs = [
+        pltpu.make_async_copy(routes_t_hbm, routes_t_ref, in_sem.at[1]),
+        pltpu.make_async_copy(expert_hbm, expert_ref, in_sem.at[2]),
+    ]
+    others = [
+        pltpu.make_async_copy(mgain_hbm, mgain_ref, in_sem.at[3]),
+        pltpu.make_async_copy(scale_hbm, scale_ref, in_sem.at[4]),
+        pltpu.make_async_copy(egain_hbm, egain_ref, in_sem.at[5]),
+        pltpu.make_async_copy(rw_t_hbm, rw_t_ref, in_sem.at[6]),
+    ]
+    weights = others + [
         pltpu.make_async_copy(w_in_hbm, w_in, w_sem.at[0]),
         pltpu.make_async_copy(gate_hbm, w_gu.at[:, 0:128], w_sem.at[1]),
         pltpu.make_async_copy(up_hbm, w_gu.at[:, 128:256], w_sem.at[2]),
         pltpu.make_async_copy(w_mix_hbm, w_mix, w_sem.at[3]),
         pltpu.make_async_copy(down_hbm, w_down, w_sem.at[4]),
     ]
-    for copy in weights:
+    for copy in inputs + [own_rows] + weights:
         copy.start()
-
-    barrier = pltpu.get_barrier_semaphore()
-
-    def greet(j, carry):
-        pl.semaphore_signal(
-            barrier, inc=1, device_id={"ep": (ep + j) % n_ep}, device_id_type=MESH
-        )
-        return carry
-
-    for peer in (to_yp, to_ym, to_xp, to_xm):
-        pl.semaphore_signal(barrier, inc=1, device_id=peer, device_id_type=MESH)
-    lax.fori_loop(1, n_ep, greet, 0)
-
-    ring[y, x, 0:rows, :] = mixer_ref[...]
+    for copy in inputs:
+        copy.wait()
+
 
     def step_of(q):
         j = q // 2
@@ -124,7 +143,8 @@
         ).astype(BF)
     ring[y, x, S0 * UNIT : S0 * UNIT + CAP, :] = outgoing[0:CAP, :]
 
-    pl.semaphore_wait(barrier, n_ep - 1 + 4)
+    own_rows.wait()
+    pl.semaphore_wait(barrier, n_ep - 1 + len(plane))
 
     def remote(src, dst, send, recv, device):
         pltpu.make_async_remote_copy(
@@ -150,6 +170,13 @@
         ring_copy(ring.at[y, x, lo], ring_sem.at[u, 0, 0], to_xm)
         ring_copy(ring.at[y, x, hi], ring_sem.at[u, 1, 0], to_ym)
 
+    def direct_a(u):
+        r = u * UNIT
+        lo, hi = pl.ds(r, 64), pl.ds(r + 64, 64)
+        for to_x, to_y in ((to_xp, to_yp), (to_xm, to_ym), (across_x, across_y)):
+            ring_copy(ring.at[y, x, lo], ring_sem.at[u, 0, 0], to_x)
+            ring_copy(ring.at[y, x, hi], ring_sem.at[u, 1, 0], to_y)
+
     def second_a(u):
         r = u * UNIT
         await_bytes(ring.at[y, x, pl.ds(r, 128)], ring_sem.at[u, 0, 0])
@@ -162,8 +189,17 @@
     def first_b(u):
         r = u * UNIT
         lo, hi = pl.ds(r, 64), pl.ds(r + 64, 64)
-        await_bytes(ring.at[y, x, lo], ring_sem.at[u, 0, 1])
-        await_bytes(ring.at[y, x, lo], ring_sem.at[u, 1, 1])
+
+        @pl.when(u < S0)
+        def _():
+            await_bytes(ring.at[y, 0:3, lo], ring_sem.at[u, 0, 0])
+            await_bytes(ring.at[y, 0:3, lo], ring_sem.at[u, 1, 0])
+
+        @pl.when(u >= S0)
+        def _():
+            await_bytes(ring.at[y, x, lo], ring_sem.at[u, 0, 1])
+            await_bytes(ring.at[y, x, lo], ring_sem.at[u, 1, 1])
+
         ring_copy(ring.at[y, :, lo], ring_sem.at[u, 0, 2], to_yp)
         ring_copy(ring.at[:, x, hi], ring_sem.at[u, 1, 2], to_xp)
         ring_copy(ring.at[y, :, lo], ring_sem.at[u, 0, 2], to_ym)
@@ -183,13 +219,8 @@
         await_bytes(ring.at[y, :, pl.ds(r, 64)], ring_sem.at[u, 0, 3])
         await_bytes(ring.at[y, :, pl.ds(r, 64)], ring_sem.at[u, 1, 3])
 
-    def peer_at(q, sign):
-        dz = (q // 2 + 1) // 2 if (q // 2) % 2 == 1 else -(q // 2 // 2)
-        other = (core + q % 2) % 2
-        return {"ep": (z + sign * dz + n_z) % n_z * 2 + other}
-
     for u in range(M0, M0 + rows // UNIT):
-        first_a(u)
+        direct_a(u)
     for q in range(1, n_ep):
         remote(
             outgoing.at[q * CAP : (q + 1) * CAP],
@@ -254,15 +285,17 @@
         both = jnp.dot(normed[...], w_gu[...], preferred_element_type=F32)
         gate, up = both[:, 0:128], both[:, 128:256]
         hidden = gate / (1.0 + jnp.exp(-gate)) * up
-        ring[y, x, pl.ds((u - S0 + H0) * UNIT, UNIT), :] = hidden.astype(BF)
+        turn = (u - S0 + SLOT_UNITS - TURN) % SLOT_UNITS
+        ring[y, x, pl.ds((turn + H0) * UNIT, UNIT), :] = hidden.astype(BF)
 
     def pooled_unit(u):
-        mixer_out[pl.ds((u - P0) * UNIT, UNIT), :] = jnp.dot(
+        out[pl.ds((u - P0) * UNIT, UNIT), :] = jnp.dot(
             wide(u), w_mix[...], preferred_element_type=F32
         ).astype(BF)
 
     def hidden_unit(u):
-        back[pl.ds((u - H0) * UNIT, UNIT), :] = jnp.dot(
+        turn = (u - H0 + TURN) % SLOT_UNITS
+        back[pl.ds(turn * UNIT, UNIT), :] = jnp.dot(
             wide(u), w_down[...], preferred_element_type=F32
         ).astype(BF)
 
@@ -342,10 +375,10 @@
         return ((u >= M0) & (u < M0 + rows // UNIT)) | ((u >= S0) & (u < UNITS))
 
     def step(i, carry):
-        for lag, stage in ((3 * LAG, second_b), (2 * LAG, first_b), (LAG, second_a)):
+        for lag, stage in ((B2, second_b), (B1, first_b), (A2, second_a)):
             u = i - lag
 
-            @pl.when(sends(u))
+            @pl.when((u >= S0) & (u < UNITS) if stage is second_a else sends(u))
             def _():
                 stage(u)
 
@@ -360,16 +393,12 @@
         def _():
             first_a(i)
 
-        @pl.when(i == S0 + 4)
-        def _():
-            place_results()
-
-        u = i - 4 * LAG
-
-        @pl.when(u == UNITS - 1)
-        def _():
-            combine(n_groups - 1)
-            expert_out[...] = (
+        u = i - DONE
+
+        @pl.when(u == UNITS - 2)
+        def _():
+            combine(0)
+            out[rows : 2 * rows, :] = (
                 picked[0:rows, :] * weight_of[0:rows, :]
                 + picked[rows : 2 * rows, :] * weight_of[rows : 2 * rows, :]
             ).astype(BF)
@@ -378,6 +407,10 @@
         def _():
             finished(u)
 
+        @pl.when(u == S0 + 2)
+        def _():
+            place_results()
+
         @pl.when(u == M0)
         def _():
             for copy in weights:
@@ -412,12 +445,12 @@
             @pl.when(u == H0 + 3 * g + 2)
             def _():
                 if g > 0:
-                    combine(g - 1)
-                send_back(g)
+                    combine(g)
+                send_back((g + 1) % n_groups)
 
         return carry
 
-    lax.fori_loop(0, UNITS + 4 * LAG, step, 0)
+    lax.fori_loop(B1, UNITS + DONE, step, 0)
     sent = (SIDE * SIDE - 1) * (2 * rows + 2 * slots) // (SIDE * SIDE)
     await_bytes(ring.at[:, :, 0:sent], send_sem)
     await_bytes(outgoing.at[0 : slots - CAP], disp_send)
@@ -445,15 +478,12 @@
     vmem = pl.BlockSpec(memory_space=pltpu.VMEM)
     hbm = pl.BlockSpec(memory_space=pl.ANY)
     slots = n_ep * CAP
-    return pl.pallas_call(
+    both = pl.pallas_call(
         kernel,
         name="mixer_and_experts",
-        out_shape=(
-            jax.ShapeDtypeStruct((rows, feats), BF),
-            jax.ShapeDtypeStruct((rows, feats), BF),
-        ),
-        in_specs=[vmem] * 7 + [hbm] * 5,
-        out_specs=(vmem, vmem),
+        out_shape=jax.ShapeDtypeStruct((2 * rows, feats), BF),
+        in_specs=[hbm] * 12,
+        out_specs=vmem,
         scratch_shapes=[
             pltpu.VMEM((SIDE, SIDE, UNITS * UNIT, feats), BF),
             pltpu.VMEM((depth, 128), BF),
@@ -470,7 +500,14 @@
             pltpu.VMEM((2 * rows, 128), F32),
             pltpu.VMEM((n_ep, rows), F32),
             pltpu.VMEM((2 * rows, feats), F32),
+            pltpu.VMEM((rows, feats), BF),
+            pltpu.VMEM((depth // 128, 128), F32),
+            pltpu.VMEM((1, feats), F32),
+            pltpu.VMEM((depth // 128, 128), F32),
+            pltpu.VMEM((2, rows), jnp.int32),
+            pltpu.VMEM((2, rows), F32),
             pltpu.SemaphoreType.DMA((5,)),
+            pltpu.SemaphoreType.DMA((7,)),
             pltpu.SemaphoreType.DMA,
             pltpu.SemaphoreType.DMA((UNITS, 2, 4)),
             pltpu.SemaphoreType.DMA,
@@ -497,6 +534,7 @@
         expert_up[0],
         expert_down[0],
     )
+    return both[0:rows], both[rows:]
 
 
 def solution(mesh):

time: 125 us -> 120 us (0.960)
  Pallas kernels: 122 us -> 117 us
    pallas_call x1, Pallas kernels: 122 us -> 117 us  [on_device(): pl.pallas_call(kernel, name='mixer_and_experts', out_shape=jax.ShapeDtype...]
    unnamed x4 -> x0, local copies, waits for them, and re-layouts: 2.26 us -> none
    slice x0 -> x1, local copies, waits for them, and re-layouts: none -> 1.69 us  [on_device(): return (both[0:rows], both[rows:])]
where the time goes in v3:
time: 120 us
  Pallas kernels  117 us (98%)
  local copies, waits for them, and re-layouts  1.69 us (1%)
    pallas_call x1, Pallas kernels, on_device(): pl.pallas_call(kernel, name='mixer_and_experts', out_shape=jax.ShapeDtype...  117 us

profile of v3, /device:TPU:1, one launch (start us, length us, event | category | flops | bytes accessed | tf_op | source)
XLA Modules:
  0.0 119.7 jit_solution(10722715202662368035)
XLA Ops:
  0.6 117.3 %mixer_and_experts.1 = bf16[1024,128]{1,0:T(8,128)(2,1)} custom-call(bf16[512,128]{1,0:T(8,128)(2,1)} %mixer_hbm.1, bf16[512,128]{1,0:T(8,128)(2,1)} %expert_hbm.1, f32[16,128]{1,0:T(8,128)} %bitcast.11, f32[1,128]{1,0:T(1,128)} %bitcast.15, f32[16,128]{1,0:T(8,128)} %bitcast.12, s32[2,512]{1,0:T(2,128)} %bitcast.13, f32[2,512]{1,0:T(2,128)} %bitcast.14, ...), custom_call_target="tpu_custom_call" | custom-call | tf_op jit(solution)/shard_map/mixer_and_experts/pallas_call | solution.py:481
  118.0 1.7 %fusion = (bf16[512,128]{1,0:T(8,128)(2,1)}, bf16[512,128]{1,0:T(8,128)(2,1)}) fusion(bf16[1024,128]{1,0:T(8,128)(2,1)} %mixer_and_experts.1), kind=kLoop, calls=%fused_computation | loop fusion | bytes 524288 | tf_op jit(solution)/shard_map/slice | solution.py:537

commit v4 on v3

--- a/solution.py
+++ b/solution.py
@@ -226,7 +226,7 @@
             outgoing.at[q * CAP : (q + 1) * CAP],
             ring.at[y, x, S0 * UNIT + q * CAP : S0 * UNIT + (q + 1) * CAP],
             disp_send,
-            disp_sem.at[q // 8],
+            disp_sem.at[q // 8 * 3 + q % 8 // 3],
             peer_at(q, 1),
         )
 
@@ -382,12 +382,16 @@
             def _():
                 stage(u)
 
-        for g in range(n_groups):
-
-            @pl.when(i == S0 + 3 * g)
+        k = i - S0
+        for first, count in ((0, 3), (1, 3), (2, 2)):
+
+            @pl.when((k > 0) & (k < SLOT_UNITS) & (k % 3 == first))
             def _():
-                count = group if g > 0 else group - CAP
-                await_bytes(ring.at[y, x, 0:count], disp_sem.at[g])
+                await_bytes(ring.at[y, x, 0 : count * CAP], disp_sem.at[k])
+
+        @pl.when(k == 0)
+        def _():
+            await_bytes(ring.at[y, x, 0 : 2 * CAP], disp_sem.at[0])
 
         @pl.when((i >= S0) & (i < UNITS))
         def _():
@@ -511,7 +515,7 @@
             pltpu.SemaphoreType.DMA,
             pltpu.SemaphoreType.DMA((UNITS, 2, 4)),
             pltpu.SemaphoreType.DMA,
-            pltpu.SemaphoreType.DMA((n_ep // 8,)),
+            pltpu.SemaphoreType.DMA((SLOT_UNITS,)),
             pltpu.SemaphoreType.DMA,
             pltpu.SemaphoreType.DMA((n_ep // 8,)),
             pltpu.SemaphoreType.DMA,

time: 120 us -> 119 us (level)
  no operation moved by 1% of the time
where the time goes in v4:
time: 119 us
  Pallas kernels  116 us (97%)
  local copies, waits for them, and re-layouts  1.69 us (1%)
    pallas_call x1, Pallas kernels, on_device(): pl.pallas_call(kernel, name='mixer_and_experts', out_shape=jax.ShapeDtype...  116 us

profile of v4, /device:TPU:1, one launch (start us, length us, event | category | flops | bytes accessed | tf_op | source)
XLA Modules:
  0.0 118.8 jit_solution(14885345396631784282)
XLA Ops:
  0.6 116.5 %mixer_and_experts.1 = bf16[1024,128]{1,0:T(8,128)(2,1)} custom-call(bf16[512,128]{1,0:T(8,128)(2,1)} %mixer_hbm.1, bf16[512,128]{1,0:T(8,128)(2,1)} %expert_hbm.1, f32[16,128]{1,0:T(8,128)} %bitcast.11, f32[1,128]{1,0:T(1,128)} %bitcast.15, f32[16,128]{1,0:T(8,128)} %bitcast.12, s32[2,512]{1,0:T(2,128)} %bitcast.13, f32[2,512]{1,0:T(2,128)} %bitcast.14, ...), custom_call_target="tpu_custom_call" | custom-call | tf_op jit(solution)/shard_map/mixer_and_experts/pallas_call | solution.py:485
  117.1 1.7 %fusion = (bf16[512,128]{1,0:T(8,128)(2,1)}, bf16[512,128]{1,0:T(8,128)(2,1)}) fusion(bf16[1024,128]{1,0:T(8,128)(2,1)} %mixer_and_experts.1), kind=kLoop, calls=%fused_computation | loop fusion | bytes 524288 | tf_op jit(solution)/shard_map/slice | solution.py:541

commit v5 on v4

--- a/solution.py
+++ b/solution.py
@@ -219,9 +219,7 @@
         await_bytes(ring.at[y, :, pl.ds(r, 64)], ring_sem.at[u, 0, 3])
         await_bytes(ring.at[y, :, pl.ds(r, 64)], ring_sem.at[u, 1, 3])
 
-    for u in range(M0, M0 + rows // UNIT):
-        direct_a(u)
-    for q in range(1, n_ep):
+    def dispatch(q):
         remote(
             outgoing.at[q * CAP : (q + 1) * CAP],
             ring.at[y, x, S0 * UNIT + q * CAP : S0 * UNIT + (q + 1) * CAP],
@@ -229,6 +227,13 @@
             disp_sem.at[q // 8 * 3 + q % 8 // 3],
             peer_at(q, 1),
         )
+
+    for q in range(1, 8):
+        dispatch(q)
+    for u in range(M0, M0 + rows // UNIT):
+        direct_a(u)
+    for q in range(8, n_ep):
+        dispatch(q)
 
     def place_results():
         e_at = expert_at(q_col)

time: 119 us -> 118 us (level)
  no operation moved by 1% of the time
where the time goes in v5:
time: 118 us
  Pallas kernels  115 us (97%)
  local copies, waits for them, and re-layouts  1.69 us (1%)
    pallas_call x1, Pallas kernels, on_device(): pl.pallas_call(kernel, name='mixer_and_experts', out_shape=jax.ShapeDtype...  115 us

profile of v5, /device:TPU:1, one launch (start us, length us, event | category | flops | bytes accessed | tf_op | source)
XLA Modules:
  0.0 117.8 jit_solution(3727987282555552720)
XLA Ops:
  0.6 115.5 %mixer_and_experts.1 = bf16[1024,128]{1,0:T(8,128)(2,1)} custom-call(bf16[512,128]{1,0:T(8,128)(2,1)} %mixer_hbm.1, bf16[512,128]{1,0:T(8,128)(2,1)} %expert_hbm.1, f32[16,128]{1,0:T(8,128)} %bitcast.11, f32[1,128]{1,0:T(1,128)} %bitcast.15, f32[16,128]{1,0:T(8,128)} %bitcast.12, s32[2,512]{1,0:T(2,128)} %bitcast.13, f32[2,512]{1,0:T(2,128)} %bitcast.14, ...), custom_call_target="tpu_custom_call" | custom-call | tf_op jit(solution)/shard_map/mixer_and_experts/pallas_call | solution.py:490
  116.1 1.7 %fusion = (bf16[512,128]{1,0:T(8,128)(2,1)}, bf16[512,128]{1,0:T(8,128)(2,1)}) fusion(bf16[1024,128]{1,0:T(8,128)(2,1)} %mixer_and_experts.1), kind=kLoop, calls=%fused_computation | loop fusion | bytes 524288 | tf_op jit(solution)/shard_map/slice | solution.py:546
